TPU v7x, 32 devices: a whole 2x2x4 slice. The times are simulated.
32 devices in a mesh: ep: 8 (over z, x), tp: 4 (over y, core).
Axes of the slice: x: 2, y: 2, z: 4, core: 2. Of those that a mesh axis runs over, the one named last changes fastest.
Arguments:
- tokens: bfloat16 [128, 2048], P('ep'), may hold values from -6 to 6
- lengths: int32 [128], P('ep'), may hold values from 1 to 1024, as said below
- key_cache: bfloat16 [128, 1024, 8, 128], P('ep', None, 'tp'), may hold values from -200 to 200
- value_cache: bfloat16 [128, 1024, 8, 128], P('ep', None, 'tp'), may hold values from -6 to 6
- attn_gain: float32 [2048], replicated, may hold values from 0.1 to 1.9
- w_query: bfloat16 [2048, 8, 128], P(None, 'tp'), may hold values from -0.1875 to 0.1875
- w_key: bfloat16 [2048, 8, 128], P(None, 'tp'), may hold values from -0.15625 to 0.15625
- w_value: bfloat16 [2048, 8, 128], P(None, 'tp'), may hold values from -0.125 to 0.125
- mix_lambda: float32 [8], P('tp'), may hold values from 0.3 to 0.8
- head_gain: float32 [128], replicated, may hold values from 0.1 to 1.9
- w_out: bfloat16 [8, 128, 2048], P('tp'), may hold values from -2.5 to 2.5
- ffn_gain: float32 [2048], replicated, may hold values from 0.1 to 1.9
- w_gate: bfloat16 [8, 2048, 2048], P('ep', None, 'tp'), may hold values from -1 to 1
- w_up: bfloat16 [8, 2048, 2048], P('ep', None, 'tp'), may hold values from -1 to 1
- w_down: bfloat16 [8, 2048, 2048], P('ep', 'tp'), may hold values from -0.046875 to 0.046875
- routes: int32 [128, 4], P('ep'), may hold values from 0 to 7, all different within a row; in each aligned block of 16 rows (0 to 15, 16 to 31, ...) at most 16 rows name the same one
- route_weights: float32 [128, 4], P('ep'), may hold values from 0.1 to 1
Outputs:
- mixed: bfloat16 [128, 2048], P('ep', 'tp')
Inputs may be any that keep to these rules, and one draw needn't show every extreme that they name: `routes`: in each aligned block of 16 rows no expert is named by more than 16 entries, and one is named by exactly 16 in some block; each row names 4 different experts. `lengths`: some sequence has all 1024 positions valid.
All inputs are finite; a program needn't handle non-finite values.
Results may differ from a plain program's by a relative error of at most 0.02.
The roundings to bfloat16 on the way count: a program that leaves them out, or rounds other values in their place, can miss the bound.
Values may be sent and summed in bfloat16 or wider, within the bound.
No kernel may reach another device: no remote copies, remote signals or barrier semaphores. Data moves between devices by JAX's collectives and lax.ppermute only.
A program may use at most 128 MiB of HBM per device.

v0:
```python
import jax
import jax.numpy as jnp
from jax import lax
from jax.sharding import PartitionSpec as P

epsilon = 1e-06
clamp_limit = 7.0
sigmoid_slope = 1.702
branch_scale = 0.2


def norm_rows(source, gain):
    wide = source.astype(jnp.float32)
    return wide * lax.rsqrt(jnp.mean(wide * wide, axis=-1, keepdims=True) + epsilon) * gain


def mixed_weights(scores, own_scores, mix_lambda):
    peak = jnp.maximum(jnp.max(scores, axis=-1), own_scores)
    weights = jnp.exp(scores - peak[..., None])
    own_weight = jnp.exp(own_scores - peak)
    denominator = jnp.sum(weights, axis=-1) + own_weight
    shares = weights / denominator[..., None]
    own_share = own_weight / denominator
    balance = mix_lambda[None, :]
    mix_weights = (shares[:, :, 0] - balance[..., None] * shares[:, :, 1]).astype(jnp.bfloat16)
    own_mixed = (own_share[:, :, 0] - balance * own_share[:, :, 1]).astype(jnp.bfloat16)
    return (mix_weights, own_mixed)


def per_device(
    tokens,
    lengths,
    key_cache,
    value_cache,
    attn_gain,
    w_query,
    w_key,
    w_value,
    mix_lambda,
    head_gain,
    w_out,
    ffn_gain,
    w_gate,
    w_up,
    w_down,
    routes,
    route_weights,
):
    seq_dev, model_width = tokens.shape
    group_heads = w_query.shape[1]
    head_width = w_query.shape[2]
    half_width = head_width // 2
    columns = group_heads * head_width
    cache_len = key_cache.shape[1]
    normed = norm_rows(tokens, attn_gain).astype(jnp.bfloat16)
    queries = (
        jnp.dot(normed, w_query.reshape(model_width, columns), preferred_element_type=jnp.float32)
        .astype(jnp.bfloat16)
        .reshape(seq_dev, group_heads, head_width)
    )
    key_new = (
        jnp.dot(normed, w_key.reshape(model_width, columns), preferred_element_type=jnp.float32)
        .astype(jnp.bfloat16)
        .reshape(seq_dev, group_heads, head_width)
    )
    value_new = (
        jnp.dot(normed, w_value.reshape(model_width, columns), preferred_element_type=jnp.float32)
        .astype(jnp.bfloat16)
        .reshape(seq_dev, group_heads, head_width)
    )
    halves = (lax.iota(jnp.int32, head_width) < half_width).astype(jnp.bfloat16)
    stacked_query = jnp.stack([queries * halves, queries * (1 - halves)], axis=2)
    score_scale = half_width ** (-0.5)
    own_scores = (
        jnp.einsum("shcd,shd->shc", stacked_query, key_new, preferred_element_type=jnp.float32)
        * score_scale
    )
    positions = lax.iota(jnp.int32, cache_len)
    live_mask = (positions[None, :] < lengths[:, None])[:, None, None, :]
    scores = (
        jnp.einsum("shcd,slhd->shcl", stacked_query, key_cache, preferred_element_type=jnp.float32)
        * score_scale
    )
    scores = jnp.where(live_mask, scores, -jnp.inf)
    mix_weights, own_mixed = mixed_weights(scores, own_scores, mix_lambda)
    heads_out = jnp.einsum(
        "shl,slhd->shd", mix_weights, value_cache, preferred_element_type=jnp.float32
    )
    heads_out = heads_out + own_mixed.astype(jnp.float32)[..., None] * value_new.astype(jnp.float32)
    normed_heads = (
        heads_out
        * lax.rsqrt(jnp.mean(heads_out * heads_out, axis=-1, keepdims=True) + epsilon)
        * head_gain
        * branch_scale
    ).astype(jnp.bfloat16)
    partial_value = jnp.dot(
        normed_heads.reshape(seq_dev, columns),
        w_out.reshape(columns, model_width),
        preferred_element_type=jnp.float32,
    )
    partial_value = lax.optimization_barrier(partial_value.astype(jnp.bfloat16)).astype(jnp.float32)
    attention = lax.psum(partial_value.astype(jnp.bfloat16), "tp").astype(jnp.float32)
    residual = (tokens.astype(jnp.float32) + attention).astype(jnp.bfloat16)
    normed_ffn = norm_rows(residual, ffn_gain).astype(jnp.bfloat16)
    experts = lax.axis_size("ep")
    top_count = routes.shape[1]
    capacity = 2 * seq_dev * top_count // experts
    entries = routes.reshape(-1)
    onehot = (entries[:, None] == lax.iota(jnp.int32, experts)[None, :]).astype(jnp.int32)
    entry_slot = jnp.sum((jnp.cumsum(onehot, axis=0) - onehot) * onehot, axis=-1)
    target = entries * capacity + entry_slot
    slot_ids = lax.iota(jnp.int32, experts * capacity)
    placing = (slot_ids[:, None] == target[None, :]).astype(jnp.bfloat16)
    repeated = jnp.repeat(normed_ffn, top_count, axis=0)
    outgoing = jnp.dot(placing, repeated, preferred_element_type=jnp.float32).astype(jnp.bfloat16)
    outgoing = outgoing.reshape(experts, capacity, model_width)
    block_cols = model_width // lax.axis_size("tp")
    own_block = lax.dynamic_slice_in_dim(outgoing, lax.axis_index("tp") * block_cols, block_cols, 2)
    arrived = lax.all_gather(
        lax.all_to_all(own_block, "ep", split_axis=0, concat_axis=0, tiled=True),
        "tp",
        axis=2,
        tiled=True,
    )
    sources, slot_count, _ = arrived.shape
    flat_rows = arrived.reshape(sources * slot_count, model_width)
    gate_value = jnp.minimum(
        jnp.dot(flat_rows, w_gate[0], preferred_element_type=jnp.float32), clamp_limit
    )
    up_value = jnp.clip(
        jnp.dot(flat_rows, w_up[0], preferred_element_type=jnp.float32), -clamp_limit, clamp_limit
    )
    activated = ((up_value + 1.0) * gate_value * jax.nn.sigmoid(sigmoid_slope * gate_value)).astype(
        jnp.bfloat16
    )
    pieces = jnp.dot(activated, w_down[0], preferred_element_type=jnp.float32)
    pieces = lax.optimization_barrier(pieces.astype(jnp.bfloat16)).astype(jnp.float32)
    summed = lax.psum_scatter(
        pieces.reshape(sources, slot_count, model_width).astype(jnp.bfloat16),
        "tp",
        scatter_dimension=2,
        tiled=True,
    )
    returned = lax.all_to_all(summed, "ep", split_axis=0, concat_axis=0, tiled=True)
    slice_width = returned.shape[2]
    returned = returned.reshape(experts * capacity, slice_width).astype(jnp.float32)
    chosen = (target.reshape(seq_dev, top_count)[..., None] == slot_ids[None, None, :]).astype(
        jnp.float32
    )
    combine = jnp.sum(route_weights[..., None] * chosen, axis=1)
    expert_sum = jnp.dot(combine, returned, precision=lax.Precision.HIGHEST)
    own_columns = lax.dynamic_slice_in_dim(
        residual, lax.axis_index("tp") * slice_width, slice_width, 1
    )
    return (own_columns.astype(jnp.float32) + expert_sum).astype(jnp.bfloat16)


def solution(mesh):
    placed = (
        P("ep", None),
        P("ep"),
        P("ep", None, "tp", None),
        P("ep", None, "tp", None),
        P(),
        P(None, "tp", None),
        P(None, "tp", None),
        P(None, "tp", None),
        P("tp"),
        P(),
        P("tp", None, None),
        P(),
        P("ep", None, "tp"),
        P("ep", None, "tp"),
        P("ep", "tp", None),
        P("ep", None),
        P("ep", None),
    )
    return jax.shard_map(
        per_device, mesh=mesh, in_specs=placed, out_specs=P("ep", "tp"), check_vma=False
    )
```

profile of v0, /device:TPU:0, one launch (start us, length us, event | category | flops | bytes accessed | tf_op | source)
XLA Modules:
  0.0 125.2 jit_solution(6556066839307545895)
XLA Ops:
  6.6 1.1 fusion.55
  7.7 1.6 %convolution_convert_fusion.4 = bf16[16,256]{1,0:T(8,128)(2,1)S(1)} fusion(bf16[256,8,2,128]{3,2,1,0:T(2,128)(2,1)} %bitcast.110, bf16[16,2048]{1,0:T(8,128)(2,1)} %param.17, f32[2048]{0:T(1024)} %param.21, f32[16]{0:T(128)S(1)} %add_rsqrt_fusion.2), kind=kOutput, calls=%fused_computation.26 | convolution fusion | flops 16912384 | bytes 1130560 | tf_op jit(solution)/shard_map/dot_general | solution.py:57
  9.3 1.6 %convolution_convert_fusion.3 = bf16[16,256]{1,0:T(8,128)(2,1)S(1)} fusion(bf16[256,8,2,128]{3,2,1,0:T(2,128)(2,1)} %bitcast.111, bf16[16,2048]{1,0:T(8,128)(2,1)} %param.17, f32[2048]{0:T(1024)} %param.21, f32[16]{0:T(128)S(1)} %add_rsqrt_fusion.2), kind=kOutput, calls=%fused_computation.25 | convolution fusion | flops 16912384 | bytes 1130560 | tf_op jit(solution)/shard_map/dot_general | solution.py:62
  11.0 0.1 fusion.90
  11.1 0.1 copy.68
  11.2 0.1 iota_compare_fusion.1
  11.3 0.0 copy-start.9
  11.3 0.0 copy-start.10
  11.3 5.8 %fusion.89 = (f32[16,2,2]{2,1,0:T(2,128)S(1)}, f32[16,2,2,1024]{3,2,1,0:T(2,128)S(1)}) fusion(bf16[16,2,2,128]{3,2,1,0:T(2,128)(2,1)S(1)} %pad_maximum_fusion, bf16[16,1024,2,128]{3,2,1,0:T(2,128)(2,1)} %param.19, pred[16,1024]{1,0:T(8,128)(4,1)S(1)} %iota_compare_fusion.1), kind=kOutput, calls=%fused_computation.105 | convolution fusion | flops 16973760 | bytes 8683776 | tf_op jit(solution)/shard_map/shcd,slhd->shcl/dot_general | solution.py:81
  17.2 0.0 copy-start.5
  17.2 0.1 copy.59
  17.3 0.1 copy.60
  17.4 0.3 fusion.51
  17.7 0.1 copy.61
  17.8 0.1 copy.62
  17.9 0.3 fusion.50
  18.2 0.2 fusion.88
  18.5 0.3 fusion.35
  18.8 0.1 bitcast_convert_fusion
  18.8 0.2 fusion.66
  19.1 4.8 %fusion = f32[16,2,1,128]{3,2,1,0:T(1,128)S(1)} fusion(bf16[16,1024,2,128]{3,2,1,0:T(2,128)(2,1)} %param.20, bf16[16,2,1024,1]{2,1,0,3:T(2,128)(2,1)S(1)} %fusion.66), kind=kOutput, calls=%fused_computation | convolution fusion | flops 8388608 | bytes 8470528 | tf_op jit(solution)/shard_map/shl,slhd->shd/dot_general | solution.py:86
  23.9 0.2 multiply_reduce_fusion
  24.1 0.9 fusion.4
  25.0 0.0 all-reduce.2.cloned.1.call-update
  25.0 0.0 reduce-scatter.2.cloned.1.call-start
  25.1 0.1 copy.65
  25.1 0.1 eq.20
  25.2 0.1 fusion.68
  25.3 0.1 reduce_window_sum.11
  25.4 0.2 select_reduce_fusion.1
  25.6 33.8 %all-reduce.2.cloned.1.call-done = bf16[16,2048]{1,0:T(8,128)(2,1)} async-done(((bf16[16,2048]{1,0:T(8,128)(2,1)}), bf16[16,2048]{1,0:T(8,128)(2,1)}) %all-reduce.2.cloned.1.call-update) | async-done | bytes 65552 | tf_op jit(solution)/shard_map/psum | solution.py:102
  59.4 1.0 fusion.52
  60.4 0.1 fusion.54
  60.5 0.1 broadcast_in_dim.16
  60.6 0.1 reshape.137
  60.7 0.3 convolution_convert_fusion.1
  61.0 12.7 %all_to_all.10 = bf16[8,16,512]{2,1,0:T(8,128)(2,1)S(1)} all-to-all(bf16[8,16,512]{2,1,0:T(8,128)(2,1)S(1)} %constant_dynamic-slice_fusion), channel_id=1, replica_groups=mesh['ep'=8,'tp'=4] {'ep'}, dimensions={0} | all-to-all | bytes 262144 | tf_op jit(solution)/shard_map/all_to_all | solution.py:120
  73.6 6.5 %all_gather.3 = bf16[8,16,2048]{2,1,0:T(8,128)(2,1)S(1)} all-gather(bf16[8,16,512]{2,1,0:T(8,128)(2,1)S(1)} %all_to_all.10), channel_id=1, replica_groups=mesh['ep'=8,'tp'=4] {'tp'}, dimensions={2}, use_global_device_ids=true | all-gather | bytes 655360 | tf_op jit(solution)/shard_map/all_gather | solution.py:119
  80.1 2.0 %fusion.13 = f32[128,512]{1,0:T(8,128)S(1)} fusion(bf16[128,2048]{1,0:T(8,128)(2,1)S(1)} %bitcast.105, bf16[1,2048,512]{2,1,0:T(8,128)(2,1)} %param.29), kind=kOutput, calls=%fused_computation.14 | convolution fusion | flops 268500992 | bytes 2883584 | tf_op jit(solution)/shard_map/dot_general | solution.py:128
  82.2 3.2 %convolution_convert_fusion = bf16[128,2048]{1,0:T(8,128)(2,1)} fusion(bf16[1,512,2048]{2,1,0:T(8,128)(2,1)S(1)} %copy-done, f32[128,512]{1,0:T(8,128)S(1)} %fusion.13, bf16[128,2048]{1,0:T(8,128)(2,1)S(1)} %bitcast.106, bf16[1,2048,512]{2,1,0:T(8,128)(2,1)} %param.30), kind=kOutput, calls=%fused_computation.4 | convolution fusion | flops 537722880 | bytes 5505024 | tf_op jit(solution)/shard_map/dot_general | solution.py:136
  85.4 0.0 reduce-scatter.2.cloned.1.call-update
  85.4 0.1 reduce_sum.60
  85.5 0.1 copy.66
  85.6 19.2 %reduce-scatter.2.cloned.1.call-done = bf16[8,16,512]{2,1,0:T(8,128)(2,1)} async-done(((bf16[8,16,2048]{2,1,0:T(8,128)(2,1)}), bf16[8,16,512]{2,1,0:T(8,128)(2,1)}) %reduce-scatter.2.cloned.1.call-update) | async-done | bytes 131088 | tf_op jit(solution)/shard_map/reduce_scatter | solution.py:138
  104.8 5.5 %all-to-all-start.1 = ((bf16[8,16,512]{2,1,0:T(8,128)(2,1)}), bf16[8,16,512]{2,1,0:T(8,128)(2,1)S(1)}, u32[]{:S(2)}, u32[]{:S(2)}) async-start(bf16[8,16,512]{2,1,0:T(8,128)(2,1)} %reduce-scatter.2.cloned.1.call-done), calls=%async_computation.2 | async-start | bytes 262144 | tf_op jit(solution)/shard_map/all_to_all | solution.py:144
  110.3 0.1 select_reduce_fusion
  110.4 7.2 %all-to-all-done.1 = bf16[8,16,512]{2,1,0:T(8,128)(2,1)S(1)} async-done(((bf16[8,16,512]{2,1,0:T(8,128)(2,1)}), bf16[8,16,512]{2,1,0:T(8,128)(2,1)S(1)}, u32[]{:S(2)}, u32[]{:S(2)}) %all-to-all-start.1) | async-done | bytes 131104 | tf_op jit(solution)/shard_map/all_to_all | solution.py:144
  117.6 0.8 fusion.33
  (34 shorter events, 0.2 us)
Async XLA Ops:
  6.5 75.6 %copy-start = (bf16[1,512,2048]{2,1,0:T(8,128)(2,1)S(1)}, bf16[1,512,2048]{2,1,0:T(8,128)(2,1)}, u32[]{:S(2)}) copy-start(bf16[1,512,2048]{2,1,0:T(8,128)(2,1)} %param.31) | copy-start | bytes 6291460
  6.5 4.7 %copy-start.8 = (s32[16]{0:T(128)S(1)}, s32[16]{0:T(128)}, u32[]{:S(2)}) copy-start(s32[16]{0:T(128)} %param.18) | copy-start | bytes 196
  6.5 52.9 %all-reduce.2.cloned.1.call-start = ((), (), s32[]{:S(2)}) async-start(), calls=%async_computation.3 | async-start | bytes 131072 | tf_op jit(solution)/shard_map/psum | solution.py:102
  11.3 7.2 %copy-start.2 = (bf16[16,2048]{1,0:T(8,128)(2,1)S(1)}, bf16[16,2048]{1,0:T(8,128)(2,1)}, u32[]{:S(2)}) copy-start(bf16[16,2048]{1,0:T(8,128)(2,1)} %param.17) | copy-start | bytes 196612
  11.3 7.2 %copy-start.9 = (bf16[2048,2,128]{2,1,0:T(2,128)(2,1)S(1)}, bf16[2048,2,128]{2,1,0:T(2,128)(2,1)}, u32[]{:S(2)}) copy-start(bf16[2048,2,128]{2,1,0:T(2,128)(2,1)} %param.24) | copy-start | bytes 3145732
  11.3 7.2 %copy-start.10 = (f32[2048]{0:T(1024)S(1)}, f32[2048]{0:T(1024)}, u32[]{:S(2)}) copy-start(f32[2048]{0:T(1024)} %param.21) | copy-start | bytes 24580
  17.2 1.6 %copy-start.5 = (f32[2]{0:T(128)S(1)}, f32[2]{0:T(128)}, u32[]{:S(2)}) copy-start(f32[2]{0:T(128)} %param.25) | copy-start | bytes 28
  19.0 5.0 %copy-start.1 = (bf16[2,128,2048]{2,1,0:T(8,128)(2,1)S(1)}, bf16[2,128,2048]{2,1,0:T(8,128)(2,1)}, u32[]{:S(2)}) copy-start(bf16[2,128,2048]{2,1,0:T(8,128)(2,1)} %param.27) | copy-start | bytes 3145732
  19.0 5.0 %copy-start.7 = (f32[128]{0:T(128)S(1)}, f32[128]{0:T(128)}, u32[]{:S(2)}) copy-start(f32[128]{0:T(128)} %param.26) | copy-start | bytes 1540
  19.0 6.0 %copy-start.4 = (s32[16,4]{0,1:T(4,128)S(1)}, s32[16,4]{0,1:T(4,128)}, u32[]{:S(2)}) copy-start(s32[16,4]{0,1:T(4,128)} %param.32) | copy-start | bytes 772
  19.1 41.3 %copy-start.3 = (f32[2048]{0:T(1024)S(1)}, f32[2048]{0:T(1024)}, u32[]{:S(2)}) copy-start(f32[2048]{0:T(1024)} %param.28) | copy-start | bytes 24580
  25.0 79.8 %reduce-scatter.2.cloned.1.call-start = ((), (), s32[]{:S(2)}) async-start(), calls=%async_computation.4 | async-start | bytes 655360 | tf_op jit(solution)/shard_map/reduce_scatter | solution.py:138
  82.2 28.1 %copy-start.6 = (f32[16,4]{0,1:T(4,128)S(1)}, f32[16,4]{0,1:T(4,128)}, u32[]{:S(2)}) copy-start(f32[16,4]{0,1:T(4,128)} %param.33) | copy-start | bytes 772
  104.8 12.8 %all-to-all-start.1 = ((bf16[8,16,512]{2,1,0:T(8,128)(2,1)}), bf16[8,16,512]{2,1,0:T(8,128)(2,1)S(1)}, u32[]{:S(2)}, u32[]{:S(2)}) async-start(bf16[8,16,512]{2,1,0:T(8,128)(2,1)} %reduce-scatter.2.cloned.1.call-done), calls=%async_computation.2 | async-start | bytes 262144 | tf_op jit(solution)/shard_map/all_to_all | solution.py:144
Sparse Core Ops, SparseCore 0:
  25.1 34.2 all-reduce.1
  85.6 19.1 reduce-scatter.1
where the time goes:
time: 126 us; the launch traced here: 125 us
  waiting for transfers between devices  60.2 us (48%)
  matrix products  21.5 us (17%)
  blocking collectives  19.1 us (15%)
  between operations  13.7 us (11%)
  starting transfers between devices  5.55 us (4%)
  other arithmetic  3.87 us (3%)
  local copies, waits for them, and re-layouts  1.29 us (1%)
    psum x1, waiting for transfers between devices, per_device(): lax.psum(partial_value.astype(jnp.bfloat16), 'tp').astype(jnp.float32)  33.8 us
    reduce_scatter x1, waiting for transfers between devices, per_device(): lax.psum_scatter(pieces.reshape(sources, slot_count, model_width).astype(...  19.2 us
    all_to_all x1, blocking collectives, per_device(): lax.all_to_all(own_block, 'ep', split_axis=0, concat_axis=0, tiled=True)  12.7 us
    all_to_all x1, waiting for transfers between devices, per_device(): lax.all_to_all(summed, 'ep', split_axis=0, concat_axis=0, tiled=True)  7.24 us
    all_gather x1, blocking collectives, per_device(): lax.all_gather(lax.all_to_all(own_block, 'ep', split_axis=0, concat_axis=...  6.49 us
    dot_general x1, matrix products, per_device(): jnp.einsum('shcd,slhd->shcl', stacked_query, key_cache, preferred_element...  5.84 us
    all_to_all x1, starting transfers between devices, per_device(): lax.all_to_all(summed, 'ep', split_axis=0, concat_axis=0, tiled=True)  5.5 us
    dot_general x1, matrix products, per_device(): jnp.einsum('shl,slhd->shd', mix_weights, value_cache, preferred_element_t...  4.8 us
  transfers between devices with their start and end apart: 3, of which 3 were waited for; matrix products, arithmetic and copies ran while one was open for 1% of the time, Pallas kernels for 0%

commit v1 on v0

--- a/solution.py
+++ b/solution.py
@@ -7,6 +7,12 @@
 clamp_limit = 7.0
 sigmoid_slope = 1.702
 branch_scale = 0.2
+
+
+def summed_here(block, mesh_axis):
+    parts = lax.all_gather(block, mesh_axis, axis=0, tiled=False)
+    total = parts.sum(axis=0)
+    return total
 
 
 def norm_rows(source, gain):
@@ -99,7 +105,7 @@
         preferred_element_type=jnp.float32,
     )
     partial_value = lax.optimization_barrier(partial_value.astype(jnp.bfloat16)).astype(jnp.float32)
-    attention = lax.psum(partial_value.astype(jnp.bfloat16), "tp").astype(jnp.float32)
+    attention = summed_here(partial_value.astype(jnp.bfloat16), "tp").astype(jnp.float32)
     residual = (tokens.astype(jnp.float32) + attention).astype(jnp.bfloat16)
     normed_ffn = norm_rows(residual, ffn_gain).astype(jnp.bfloat16)
     experts = lax.axis_size("ep")

time: 126 us -> 98.9 us (0.78)
  waiting for transfers between devices: 60.2 us -> 26.6 us
  blocking collectives: 19.1 us -> 27.5 us
    psum x1 -> x0, waiting for transfers between devices: 33.8 us -> none  [per_device(): lax.psum(partial_value.astype(jnp.bfloat16), 'tp').astype(jnp.float32)]
    all_gather x0 -> x1, blocking collectives: none -> 7.25 us  [summed_here(): parts = lax.all_gather(block, mesh_axis, axis=0, tiled=False)]
  transfers between devices with their start and end apart: 3 -> 2, of which waited for: 3 -> 2; matrix products, arithmetic and copies ran while one was open for 1% -> 0% of each run, Pallas kernels for 0% -> 0%
where the time goes in v1:
time: 98.9 us; the launch traced here: 98.6 us
  blocking collectives  27.5 us (28%)
  waiting for transfers between devices  26.6 us (27%)
  matrix products  20.9 us (21%)
  between operations  13.7 us (14%)
  starting transfers between devices  5.51 us (6%)
  other arithmetic  3.08 us (3%)
  local copies, waits for them, and re-layouts  1.28 us (1%)
    reduce_scatter x1, waiting for transfers between devices, per_device(): lax.psum_scatter(pieces.reshape(sources, slot_count, model_width).astype(...  19.3 us
    all_to_all x1, blocking collectives, per_device(): lax.all_to_all(own_block, 'ep', split_axis=0, concat_axis=0, tiled=True)  13.1 us
    all_gather x1, blocking collectives, summed_here(): parts = lax.all_gather(block, mesh_axis, axis=0, tiled=False)  7.25 us
    all_to_all x1, waiting for transfers between devices, per_device(): lax.all_to_all(summed, 'ep', split_axis=0, concat_axis=0, tiled=True)  7.24 us
    all_gather x1, blocking collectives, per_device(): lax.all_gather(lax.all_to_all(own_block, 'ep', split_axis=0, concat_axis=...  7.19 us
    dot_general x1, matrix products, per_device(): jnp.einsum('shcd,slhd->shcl', stacked_query, key_cache, preferred_element...  5.84 us
    all_to_all x1, starting transfers between devices, per_device(): lax.all_to_all(summed, 'ep', split_axis=0, concat_axis=0, tiled=True)  5.51 us
    dot_general x1, matrix products, per_device(): jnp.einsum('shl,slhd->shd', mix_weights, value_cache, preferred_element_t...  4.8 us
  transfers between devices with their start and end apart: 2, of which 2 were waited for; matrix products, arithmetic and copies ran while one was open for 0% of the time, Pallas kernels for 0%

profile of v1, /device:TPU:0, one launch (start us, length us, event | category | flops | bytes accessed | tf_op | source)
XLA Modules:
  0.0 98.6 jit_solution(4653368464016129045)
XLA Ops:
  6.6 1.1 %fusion.55 = f32[16]{0:T(128)S(1)} fusion(bf16[16,2048]{1,0:T(8,128)(2,1)} %param.17), kind=kLoop, calls=%fused_computation.50 | loop fusion | flops 98288 | bytes 65600 | tf_op jit(solution)/shard_map/reduce_sum | solution.py:20
  7.7 1.6 %convolution_convert_fusion.4 = bf16[16,256]{1,0:T(8,128)(2,1)S(1)} fusion(bf16[256,8,2,128]{3,2,1,0:T(2,128)(2,1)} %bitcast.112, bf16[16,2048]{1,0:T(8,128)(2,1)} %param.17, f32[2048]{0:T(1024)} %param.21, f32[16]{0:T(128)S(1)} %add_rsqrt_fusion.2), kind=kOutput, calls=%fused_computation.26 | convolution fusion | flops 16912384 | bytes 1130560 | tf_op jit(solution)/shard_map/dot_general | solution.py:63
  9.3 1.6 %convolution_convert_fusion.3 = bf16[16,256]{1,0:T(8,128)(2,1)S(1)} fusion(bf16[256,8,2,128]{3,2,1,0:T(2,128)(2,1)} %bitcast.113, bf16[16,2048]{1,0:T(8,128)(2,1)} %param.17, f32[2048]{0:T(1024)} %param.21, f32[16]{0:T(128)S(1)} %add_rsqrt_fusion.2), kind=kOutput, calls=%fused_computation.25 | convolution fusion | flops 16912384 | bytes 1130560 | tf_op jit(solution)/shard_map/dot_general | solution.py:68
  11.0 0.1 fusion.90
  11.1 0.1 copy.68
  11.2 0.1 iota_compare_fusion.1
  11.3 0.0 copy-start.2
  11.3 0.0 copy-start.9
  11.3 0.0 copy-start.10
  11.3 5.8 %fusion.89 = (f32[16,2,2]{2,1,0:T(2,128)S(1)}, f32[16,2,2,1024]{3,2,1,0:T(2,128)S(1)}) fusion(bf16[16,2,2,128]{3,2,1,0:T(2,128)(2,1)S(1)} %pad_maximum_fusion, bf16[16,1024,2,128]{3,2,1,0:T(2,128)(2,1)} %param.19, pred[16,1024]{1,0:T(8,128)(4,1)S(1)} %iota_compare_fusion.1), kind=kOutput, calls=%fused_computation.105 | convolution fusion | flops 16973760 | bytes 8683776 | tf_op jit(solution)/shard_map/shcd,slhd->shcl/dot_general | solution.py:87
  17.2 0.0 copy-start.5
  17.2 0.1 copy.59
  17.3 0.1 copy.60
  17.4 0.3 fusion.51
  17.7 0.1 copy.61
  17.8 0.1 copy.62
  17.9 0.3 fusion.50
  18.2 0.2 fusion.88
  18.5 0.3 fusion.35
  18.8 0.1 bitcast_convert_fusion
  18.9 0.2 fusion.66
  19.0 0.0 copy-start.3
  19.1 4.8 %fusion = f32[16,2,1,128]{3,2,1,0:T(1,128)S(1)} fusion(bf16[16,1024,2,128]{3,2,1,0:T(2,128)(2,1)} %param.20, bf16[16,2,1024,1]{2,1,0,3:T(2,128)(2,1)S(1)} %fusion.66), kind=kOutput, calls=%fused_computation | convolution fusion | flops 8388608 | bytes 8470528 | tf_op jit(solution)/shard_map/shl,slhd->shd/dot_general | solution.py:92
  23.9 0.2 multiply_reduce_fusion
  24.0 0.3 fusion.4
  24.3 7.2 %all-gather = bf16[64,2048]{1,0:T(8,128)(2,1)S(1)} all-gather(bf16[16,2048]{1,0:T(8,128)(2,1)S(1)} %fusion.4), channel_id=2, replica_groups=mesh['ep'=8,'tp'=4] {'tp'}, dimensions={0}, use_global_device_ids=true | all-gather | bytes 327680 | tf_op jit(solution)/shard_map/all_gather | solution.py:13
  31.6 0.1 fusion.52
  31.8 0.1 fusion.54
  31.9 0.1 broadcast_in_dim.16
  32.0 0.1 reshape.137
  32.1 0.1 copy.65
  32.1 0.1 eq.20
  32.2 0.1 fusion.68
  32.3 0.1 reduce_window_sum.11
  32.4 0.2 select_reduce_fusion.1
  32.6 0.3 convolution_convert_fusion.1
  32.9 13.1 %all_to_all.10 = bf16[8,16,512]{2,1,0:T(8,128)(2,1)S(1)} all-to-all(bf16[8,16,512]{2,1,0:T(8,128)(2,1)S(1)} %constant_dynamic-slice_fusion), channel_id=1, replica_groups=mesh['ep'=8,'tp'=4] {'ep'}, dimensions={0} | all-to-all | bytes 262144 | tf_op jit(solution)/shard_map/all_to_all | solution.py:126
  46.0 7.2 %all_gather.11 = bf16[8,16,2048]{2,1,0:T(8,128)(2,1)S(1)} all-gather(bf16[8,16,512]{2,1,0:T(8,128)(2,1)S(1)} %all_to_all.10), channel_id=1, replica_groups=mesh['ep'=8,'tp'=4] {'tp'}, dimensions={2}, use_global_device_ids=true | all-gather | bytes 655360 | tf_op jit(solution)/shard_map/all_gather | solution.py:125
  53.2 2.1 %fusion.13 = f32[128,512]{1,0:T(8,128)S(1)} fusion(bf16[128,2048]{1,0:T(8,128)(2,1)S(1)} %bitcast.106, bf16[1,2048,512]{2,1,0:T(8,128)(2,1)} %param.29), kind=kOutput, calls=%fused_computation.14 | convolution fusion | flops 268500992 | bytes 2883584 | tf_op jit(solution)/shard_map/dot_general | solution.py:134
  55.3 3.3 %convolution_convert_fusion = bf16[128,2048]{1,0:T(8,128)(2,1)} fusion(bf16[1,512,2048]{2,1,0:T(8,128)(2,1)S(1)} %copy-done, f32[128,512]{1,0:T(8,128)S(1)} %fusion.13, bf16[128,2048]{1,0:T(8,128)(2,1)S(1)} %bitcast.107, bf16[1,2048,512]{2,1,0:T(8,128)(2,1)} %param.30), kind=kOutput, calls=%fused_computation.4 | convolution fusion | flops 537722880 | bytes 5505024 | tf_op jit(solution)/shard_map/dot_general | solution.py:142
  58.6 0.0 reduce-scatter.2.cloned.1.call-update
  58.6 0.1 reduce_sum.73
  58.7 0.1 copy.66
  58.8 19.3 %reduce-scatter.2.cloned.1.call-done = bf16[8,16,512]{2,1,0:T(8,128)(2,1)} async-done(((bf16[8,16,2048]{2,1,0:T(8,128)(2,1)}), bf16[8,16,512]{2,1,0:T(8,128)(2,1)}) %reduce-scatter.2.cloned.1.call-update) | async-done | bytes 131088 | tf_op jit(solution)/shard_map/reduce_scatter | solution.py:144
  78.1 5.5 %all-to-all-start.1 = ((bf16[8,16,512]{2,1,0:T(8,128)(2,1)}), bf16[8,16,512]{2,1,0:T(8,128)(2,1)S(1)}, u32[]{:S(2)}, u32[]{:S(2)}) async-start(bf16[8,16,512]{2,1,0:T(8,128)(2,1)} %reduce-scatter.2.cloned.1.call-done), calls=%async_computation.2 | async-start | bytes 262144 | tf_op jit(solution)/shard_map/all_to_all | solution.py:150
  83.6 0.1 select_reduce_fusion
  83.7 7.2 %all-to-all-done.1 = bf16[8,16,512]{2,1,0:T(8,128)(2,1)S(1)} async-done(((bf16[8,16,512]{2,1,0:T(8,128)(2,1)}), bf16[8,16,512]{2,1,0:T(8,128)(2,1)S(1)}, u32[]{:S(2)}, u32[]{:S(2)}) %all-to-all-start.1) | async-done | bytes 131104 | tf_op jit(solution)/shard_map/all_to_all | solution.py:150
  90.9 0.8 fusion.33
  (33 shorter events, 0.3 us)
Async XLA Ops:
  6.5 48.8 %copy-start = (bf16[1,512,2048]{2,1,0:T(8,128)(2,1)S(1)}, bf16[1,512,2048]{2,1,0:T(8,128)(2,1)}, u32[]{:S(2)}) copy-start(bf16[1,512,2048]{2,1,0:T(8,128)(2,1)} %param.31) | copy-start | bytes 6291460
  6.5 4.7 %copy-start.8 = (s32[16]{0:T(128)S(1)}, s32[16]{0:T(128)}, u32[]{:S(2)}) copy-start(s32[16]{0:T(128)} %param.18) | copy-start | bytes 196
  6.5 71.5 %reduce-scatter.2.cloned.1.call-start = ((), (), s32[]{:S(2)}) async-start(), calls=%async_computation.3 | async-start | bytes 655360 | tf_op jit(solution)/shard_map/reduce_scatter | solution.py:144
  11.3 7.2 %copy-start.2 = (bf16[16,2048]{1,0:T(8,128)(2,1)S(1)}, bf16[16,2048]{1,0:T(8,128)(2,1)}, u32[]{:S(2)}) copy-start(bf16[16,2048]{1,0:T(8,128)(2,1)} %param.17) | copy-start | bytes 196612
  11.3 7.2 %copy-start.9 = (bf16[2048,2,128]{2,1,0:T(2,128)(2,1)S(1)}, bf16[2048,2,128]{2,1,0:T(2,128)(2,1)}, u32[]{:S(2)}) copy-start(bf16[2048,2,128]{2,1,0:T(2,128)(2,1)} %param.24) | copy-start | bytes 3145732
  11.3 7.2 %copy-start.10 = (f32[2048]{0:T(1024)S(1)}, f32[2048]{0:T(1024)}, u32[]{:S(2)}) copy-start(f32[2048]{0:T(1024)} %param.21) | copy-start | bytes 24580
  17.2 1.6 %copy-start.5 = (f32[2]{0:T(128)S(1)}, f32[2]{0:T(128)}, u32[]{:S(2)}) copy-start(f32[2]{0:T(128)} %param.25) | copy-start | bytes 28
  19.0 5.0 %copy-start.1 = (bf16[2,128,2048]{2,1,0:T(8,128)(2,1)S(1)}, bf16[2,128,2048]{2,1,0:T(8,128)(2,1)}, u32[]{:S(2)}) copy-start(bf16[2,128,2048]{2,1,0:T(8,128)(2,1)} %param.27) | copy-start | bytes 3145732
  19.0 5.0 %copy-start.7 = (f32[128]{0:T(128)S(1)}, f32[128]{0:T(128)}, u32[]{:S(2)}) copy-start(f32[128]{0:T(128)} %param.26) | copy-start | bytes 1540
  19.0 12.7 %copy-start.3 = (f32[2048]{0:T(1024)S(1)}, f32[2048]{0:T(1024)}, u32[]{:S(2)}) copy-start(f32[2048]{0:T(1024)} %param.28) | copy-start | bytes 24580
  23.9 8.2 %copy-start.4 = (s32[16,4]{0,1:T(4,128)S(1)}, s32[16,4]{0,1:T(4,128)}, u32[]{:S(2)}) copy-start(s32[16,4]{0,1:T(4,128)} %param.32) | copy-start | bytes 772
  55.3 28.3 %copy-start.6 = (f32[16,4]{0,1:T(4,128)S(1)}, f32[16,4]{0,1:T(4,128)}, u32[]{:S(2)}) copy-start(f32[16,4]{0,1:T(4,128)} %param.33) | copy-start | bytes 772
  78.1 12.9 %all-to-all-start.1 = ((bf16[8,16,512]{2,1,0:T(8,128)(2,1)}), bf16[8,16,512]{2,1,0:T(8,128)(2,1)S(1)}, u32[]{:S(2)}, u32[]{:S(2)}) async-start(bf16[8,16,512]{2,1,0:T(8,128)(2,1)} %reduce-scatter.2.cloned.1.call-done), calls=%async_computation.2 | async-start | bytes 262144 | tf_op jit(solution)/shard_map/all_to_all | solution.py:150
Sparse Core Ops, SparseCore 0:
  58.7 19.3 reduce-scatter.1
